TPU v7x, 32 devices: a whole 2x2x4 slice. The times are simulated.
32 devices in a mesh: grp: 2 (over y), tp: 4 (over z), dp: 4 (over x, core).
Axes of the slice: x: 2, y: 2, z: 4, core: 2. Of those that a mesh axis runs over, the one named last changes fastest.
Arguments:
- hidden_in: bfloat16 [96, 4096], P(('grp', 'tp'), 'dp'), parts along dimension 0, may hold values from -40 to 40
- input_norm_gain: float32 [2, 4096], P(None, 'dp'), may hold values from 0.1 to 1.9
- w_query: bfloat16 [2, 4096, 2048], P(None, 'dp', 'tp'), may hold values from -0.09375 to 0.09375
- w_key: bfloat16 [2, 4096, 2048], P(None, 'dp', 'tp'), may hold values from -0.09375 to 0.09375
- w_decay: bfloat16 [2, 4096, 2048], P(None, 'dp', 'tp'), may hold values from -0.375 to 0.375
- w_value: bfloat16 [2, 4096, 4096], P(None, 'dp', 'tp'), may hold values from -0.09375 to 0.09375
- w_gate: bfloat16 [2, 4096, 4096], P(None, 'dp', 'tp'), may hold values from -0.09375 to 0.09375
- out_gain: float32 [2, 4096], P(None, 'tp'), may hold values from 0.1 to 1.9
- w_out: bfloat16 [2, 4096, 4096], P(None, 'tp', 'dp'), may hold values from -0.09375 to 0.09375
- decay_offset: float32 [2, 96, 2048], P(None, ('grp', 'dp'), 'tp'), parts along dimension 1, may hold values from -0.7 to 0
- state: float32 [2, 96, 32, 64, 128], P(None, ('grp', 'dp'), 'tp'), parts along dimension 1, may hold values from -3 to 3
Outputs:
- hidden_out: bfloat16 [96, 4096], P(('grp', 'tp'), 'dp'), parts along dimension 0
- new_state: float32 [2, 96, 32, 64, 128], P(None, ('grp', 'dp'), 'tp'), parts along dimension 1
There are 2 independent parts, one for each index of `grp`. A program takes and returns all parts, laid end to end along the dimension named above; an argument that names none is the same for every part. Nothing has to cross between parts.
All inputs are finite; a program needn't handle non-finite values.
Results may differ from a plain program's by a relative error of at most 0.017.
Values may be sent and summed in bfloat16 or wider, within the bound.
A program may use at most 64 MiB of HBM per device.

v0:
```python
import jax
import jax.numpy as jnp
from jax import lax
from jax.sharding import PartitionSpec as P

D = 4096
HEAD_KEY = 64
VALUE_CHANNELS = 128
LAYERS = 2


epsilon = 1e-06
softness_factor = 16.0


def split_heads_sum(head_terms, current):
    own_part = lax.psum_scatter(
        head_terms.astype(jnp.bfloat16), "tp", scatter_dimension=0, tiled=True
    ).astype(jnp.float32)
    return (current.astype(jnp.float32) + own_part).astype(jnp.bfloat16)


def per_device(
    hidden_in,
    input_norm_gain,
    w_query,
    w_key,
    w_decay,
    w_value,
    w_gate,
    out_gain,
    w_out,
    decay_offset,
    state,
):
    seq_rows = state.shape[1]
    local_heads = state.shape[2]
    key_cols = local_heads * HEAD_KEY
    value_cols = local_heads * VALUE_CHANNELS
    seq_start = lax.axis_index("dp") * seq_rows
    current = hidden_in
    gathered = None
    states = []
    for index_of_block in range(LAYERS):
        gathered = lax.all_gather(current, "tp", axis=0, tiled=True)
        widened = gathered.astype(jnp.float32)
        squares = jnp.sum(widened * widened, axis=1)
        scaled_query = (widened * input_norm_gain[index_of_block][None, :]).astype(jnp.bfloat16)
        partial_value = jnp.concatenate(
            [
                jnp.dot(scaled_query, matrix[index_of_block], preferred_element_type=jnp.float32)
                for matrix in (w_query, w_key, w_decay, w_value, w_gate)
            ],
            axis=1,
        ).astype(jnp.bfloat16)
        summed = lax.psum_scatter(partial_value, "dp", scatter_dimension=0, tiled=True).astype(
            jnp.float32
        )
        whole_squares = lax.psum(squares, "dp")
        own_squares = lax.dynamic_slice_in_dim(whole_squares, seq_start, seq_rows)
        inverse = lax.rsqrt(own_squares / D + epsilon)[:, None]
        projected = summed * inverse
        query_rows = projected[:, :key_cols].reshape(seq_rows, local_heads, HEAD_KEY)
        key_rows = projected[:, key_cols : 2 * key_cols].reshape(
            seq_rows, local_heads, HEAD_KEY
        ) * HEAD_KEY ** (-0.5)
        decay_logits = projected[:, 2 * key_cols : 3 * key_cols]
        value_rows = projected[:, 3 * key_cols : 3 * key_cols + value_cols].reshape(
            seq_rows, local_heads, VALUE_CHANNELS
        )
        gate_rows = projected[:, 3 * key_cols + value_cols :].reshape(
            seq_rows, local_heads, VALUE_CHANNELS
        )
        decay_logarithm = (
            jax.nn.log_sigmoid(decay_logits) / softness_factor + decay_offset[index_of_block]
        )
        decay_rate = jnp.exp(decay_logarithm).reshape(seq_rows, local_heads, HEAD_KEY)
        fresh = (
            decay_rate[:, :, :, None] * state[index_of_block]
            + key_rows[:, :, :, None] * value_rows[:, :, None, :]
        )
        readout = jnp.sum(query_rows[:, :, :, None] * fresh, axis=2)
        normed = readout * lax.rsqrt(jnp.mean(readout * readout, axis=2, keepdims=True) + epsilon)
        normed = normed * out_gain[index_of_block].reshape(local_heads, VALUE_CHANNELS)[None]
        gated_out = (
            (normed * jax.nn.silu(gate_rows)).reshape(seq_rows, value_cols).astype(jnp.bfloat16)
        )
        out_matrix = w_out[index_of_block]
        head_terms = jnp.dot(
            lax.all_gather(gated_out, "dp", axis=0, tiled=True),
            out_matrix,
            preferred_element_type=jnp.float32,
        )
        current = split_heads_sum(head_terms, current)
        gathered = None
        states.append(fresh)
    return (current, jnp.stack(states))


def solution(mesh):
    return jax.shard_map(
        per_device,
        mesh=mesh,
        in_specs=(
            P(("grp", "tp"), "dp"),
            P(None, "dp"),
            P(None, "dp", "tp"),
            P(None, "dp", "tp"),
            P(None, "dp", "tp"),
            P(None, "dp", "tp"),
            P(None, "dp", "tp"),
            P(None, "tp"),
            P(None, "tp", "dp"),
            P(None, ("grp", "dp"), "tp"),
            P(None, ("grp", "dp"), "tp", None, None),
        ),
        out_specs=(P(("grp", "tp"), "dp"), P(None, ("grp", "dp"), "tp", None, None)),
        check_vma=False,
    )
```

profile of v0, /device:TPU:0, one launch (start us, length us, event | category | flops | bytes accessed | tf_op | source)
XLA Modules:
  0.0 160.1 jit_solution(18155565338965317795)
XLA Ops:
  1.4 15.3 %all-gather = bf16[4,12,1024]{2,1,0:T(8,128)(2,1)S(1)} all-gather(bf16[1,12,1024]{2,1,0:T(8,128)(2,1)} %bitcast.127), channel_id=1, replica_groups=mesh['grp'=2,'tp'=4,'dp'=4] {'tp'}, dimensions={0}, use_global_device_ids=true | all-gather | bytes 122880 | tf_op jit(solution)/shard_map/all_gather | solution.py:45
  16.9 1.7 %fusion.63 = bf16[48,3584]{1,0:T(8,128)(2,1)S(1)} fusion(bf16[48,1024]{1,0:T(8,128)(2,1)S(1)} %get-tuple-element.13, bf16[2,1024,512]{2,1,0:T(8,128)(2,1)} %param.13), kind=kOutput, calls=%fused_computation.50 | convolution fusion | flops 50356224 | bytes 1196032 | tf_op jit(solution)/shard_map/dot_general | solution.py:51
  20.1 1.5 fusion.61
  21.6 2.1 %fusion.31 = bf16[48,3584]{1,0:T(8,128)(2,1)S(1)} fusion(bf16[48,3584]{1,0:T(8,128)(2,1)S(1)} %fusion.61, bf16[48,1024]{1,0:T(8,128)(2,1)S(1)} %get-tuple-element.13, bf16[2,1024,1024]{2,1,0:T(8,128)(2,1)} %param.16), kind=kOutput, calls=%fused_computation.30 | convolution fusion | flops 100712448 | bytes 2293760 | tf_op jit(solution)/shard_map/dot_general | solution.py:51
  24.2 10.1 %fusion = bf16[16,3584]{1,0:T(8,128)(2,1)S(1)} fusion(bf16[48,3584]{1,0:T(8,128)(2,1)S(1)} %fusion.37), kind=kCustom, calls=%all-reduce-scatter | all-reduce-scatter fusion | flops 229377 | bytes 459264
  35.8 6.9 %psum.14 = f32[48]{0:T(128)S(1)} all-reduce(f32[48]{0:T(128)S(1)} %get-tuple-element.12), channel_id=1, replica_groups=mesh['grp'=2,'tp'=4,'dp'=4] {'dp'}, use_global_device_ids=true, to_apply=%region_2.0 | all-reduce | flops 48 | bytes 384 | tf_op jit(solution)/shard_map/psum | solution.py:59
  44.8 5.2 %fusion.9 = f32[12,8,128]{2,1,0:T(8,128)S(1)} fusion(f32[2,12,8,64,128]{4,3,2,1,0:T(8,128)} %param.21, f32[12,8,128]{2,1,0:T(8,128)S(1)} %slice.134, f32[12,8,64]{2,1,0:T(8,128)S(1)} %mul.253, f32[12,8,64]{2,1,0:T(8,128)S(1)} %mul.249, f32[12,8,64]{2,1,0:T(8,128)S(1)} %mul.247), kind=kLoop, calls=%fused_computation.8 | loop fusion | flops 3919872 | bytes 3317760 | tf_op jit(solution)/shard_map/reduce_sum | solution.py:82
  50.2 5.4 %all-gather.1 = bf16[4,12,1024]{2,1,0:T(8,128)(2,1)S(1)} all-gather(bf16[1,12,1024]{2,1,0:T(8,128)(2,1)S(1)} %fusion.84), channel_id=1, replica_groups=mesh['grp'=2,'tp'=4,'dp'=4] {'dp'}, dimensions={0}, use_global_device_ids=true | all-gather | bytes 122880 | tf_op jit(solution)/shard_map/all_gather | solution.py:90
  55.7 2.1 %fusion.40 = bf16[48,1024]{1,0:T(8,128)(2,1)S(1)} fusion(bf16[48,1024]{1,0:T(8,128)(2,1)S(1)} %reshape.69, bf16[2,1024,1024]{2,1,0:T(8,128)(2,1)} %param.19), kind=kOutput, calls=%fused_computation.33 | convolution fusion | flops 100712448 | bytes 2293760 | tf_op jit(solution)/shard_map/dot_general | solution.py:89
  57.8 13.4 %fusion.1 = bf16[16,1024]{1,0:T(8,128)(2,1)S(1)} fusion(bf16[48,1024]{1,0:T(8,128)(2,1)S(1)} %fusion.40), kind=kCustom, calls=%all-reduce-scatter.1 | all-reduce-scatter fusion | flops 65537 | bytes 131584
  71.2 1.8 %collective-permute-start.1 = (bf16[12,1024]{1,0:T(8,128)(2,1)S(1)}, bf16[12,1024]{1,0:T(8,128)(2,1)S(1)}, u32[]{:S(2)}, u32[]{:S(2)}) collective-permute-start(bf16[12,1024]{1,0:T(8,128)(2,1)S(1)} %slice.131), channel_id=1, source_target_pairs={{0,4},{4,8},{8,12},{1,5},{5,9},{9,13},{2,6},{6,10},{10,14},{3,7},{... | collective-permute-start | bytes 73736
  74.7 13.4 %all-gather.2 = bf16[4,12,1024]{2,1,0:T(8,128)(2,1)S(1)} all-gather(bf16[1,12,1024]{2,1,0:T(8,128)(2,1)S(1)} %fusion.86), channel_id=1, replica_groups=mesh['grp'=2,'tp'=4,'dp'=4] {'tp'}, dimensions={0}, use_global_device_ids=true | all-gather | bytes 122880 | tf_op jit(solution)/shard_map/all_gather | solution.py:45
  88.3 5.7 %psum.15 = f32[48]{0:T(128)S(1)} all-reduce(f32[48]{0:T(128)S(1)} %get-tuple-element.10), channel_id=1, replica_groups=mesh['grp'=2,'tp'=4,'dp'=4] {'dp'}, use_global_device_ids=true, to_apply=%region_8.9 | all-reduce | flops 48 | bytes 384 | tf_op jit(solution)/shard_map/psum | solution.py:59
  94.0 1.7 %fusion.60 = bf16[48,3584]{1,0:T(8,128)(2,1)S(1)} fusion(bf16[48,1024]{1,0:T(8,128)(2,1)S(1)} %get-tuple-element.11, bf16[2,1024,512]{2,1,0:T(8,128)(2,1)} %param.13), kind=kOutput, calls=%fused_computation.44 | convolution fusion | flops 50356224 | bytes 1196032 | tf_op jit(solution)/shard_map/dot_general | solution.py:51
  97.2 1.5 fusion.58
  98.7 2.1 %fusion.46 = bf16[48,3584]{1,0:T(8,128)(2,1)S(1)} fusion(bf16[48,3584]{1,0:T(8,128)(2,1)S(1)} %fusion.58, bf16[48,1024]{1,0:T(8,128)(2,1)S(1)} %get-tuple-element.11, bf16[2,1024,1024]{2,1,0:T(8,128)(2,1)} %param.16), kind=kOutput, calls=%fused_computation.35 | convolution fusion | flops 100712448 | bytes 2293760 | tf_op jit(solution)/shard_map/dot_general | solution.py:51
  101.3 10.4 %fusion.2 = bf16[16,3584]{1,0:T(8,128)(2,1)S(1)} fusion(bf16[48,3584]{1,0:T(8,128)(2,1)S(1)} %fusion.52), kind=kCustom, calls=%all-reduce-scatter.2 | all-reduce-scatter fusion | flops 229377 | bytes 459264
  114.7 9.5 %multiply_add_fusion.1 = (f32[1,12,8,64,128]{4,3,2,1,0:T(8,128)}, f32[1,12,8,64,128]{4,3,2,1,0:T(8,128)}) fusion(f32[2,12,8,64,128]{4,3,2,1,0:T(8,128)} %param.21, f32[12,8,128]{2,1,0:T(8,128)S(1)} %slice.134, f32[12,8,64]{2,1,0:T(8,128)S(1)} %mul.253, f32[12,8,64]{2,1,0:T(8,128)S(1)} %mul.249, f32[12,8,128]{2,1,0:T(8,128)S(1)} %slice.135, ...), kind=kLoop, calls=%fused_computation.10 | loop fusion | flops 4718592 | bytes 12779520 | tf_op jit(solution)/shard_map/add | solution.py:79
  124.2 3.2 %fusion.6 = f32[12,8,128]{2,1,0:T(8,128)S(1)} fusion(f32[2,12,8,64,128]{4,3,2,1,0:T(8,128)S(1)} %bitcast.126, f32[12,8,128]{2,1,0:T(8,128)S(1)} %slice.135, f32[12,8,64]{2,1,0:T(8,128)S(1)} %mul.280, f32[12,8,64]{2,1,0:T(8,128)S(1)} %mul.276, f32[12,8,64]{2,1,0:T(8,128)S(1)} %mul.274), kind=kLoop, calls=%fused_computation.4 | loop fusion | flops 3919872 | bytes 3317760 | tf_op jit(solution)/shard_map/reduce_sum | solution.py:82
  127.7 8.9 %all-gather.3 = bf16[4,12,1024]{2,1,0:T(8,128)(2,1)S(1)} all-gather(bf16[1,12,1024]{2,1,0:T(8,128)(2,1)S(1)} %fusion.85), channel_id=1, replica_groups=mesh['grp'=2,'tp'=4,'dp'=4] {'dp'}, dimensions={0}, use_global_device_ids=true | all-gather | bytes 122880 | tf_op jit(solution)/shard_map/all_gather | solution.py:90
  136.6 2.1 %fusion.55 = bf16[48,1024]{1,0:T(8,128)(2,1)S(1)} fusion(bf16[48,1024]{1,0:T(8,128)(2,1)S(1)} %reshape.73, bf16[2,1024,1024]{2,1,0:T(8,128)(2,1)} %param.19), kind=kOutput, calls=%fused_computation.38 | convolution fusion | flops 100712448 | bytes 2293760 | tf_op jit(solution)/shard_map/dot_general | solution.py:89
  138.7 13.4 %fusion.3 = bf16[16,1024]{1,0:T(8,128)(2,1)S(1)} fusion(bf16[48,1024]{1,0:T(8,128)(2,1)S(1)} %fusion.55), kind=kCustom, calls=%all-reduce-scatter.3 | all-reduce-scatter fusion | flops 65537 | bytes 131584
  152.1 1.8 %collective-permute-start.3 = (bf16[12,1024]{1,0:T(8,128)(2,1)S(1)}, bf16[12,1024]{1,0:T(8,128)(2,1)S(1)}, u32[]{:S(2)}, u32[]{:S(2)}) collective-permute-start(bf16[12,1024]{1,0:T(8,128)(2,1)S(1)} %slice.133), channel_id=1, source_target_pairs={{0,4},{4,8},{8,12},{1,5},{5,9},{9,13},{2,6},{6,10},{10,14},{3,7},{... | collective-permute-start | bytes 73736
  153.9 5.4 %pad_maximum_fusion = f32[2,12,8,64,128]{4,3,2,1,0:T(8,128)} fusion(f32[1,12,8,64,128]{4,3,2,1,0:T(8,128)} %get-tuple-element.3, f32[1,12,8,64,128]{4,3,2,1,0:T(8,128)S(1)} %copy-done), kind=kLoop, calls=%fused_computation | loop fusion | flops 1572864 | bytes 12582912 | tf_op jit(solution)/shard_map/stack | solution.py:97
  (82 shorter events, 13.2 us)
Async XLA Ops:
  16.9 6.8 %copy-start.6 = (bf16[2,1024,1024]{2,1,0:T(8,128)(2,1)S(1)}, bf16[2,1024,1024]{2,1,0:T(8,128)(2,1)}, u32[]{:S(2)}) copy-start(bf16[2,1024,1024]{2,1,0:T(8,128)(2,1)} %param.17) | copy-start | bytes 12582916
  20.1 15.6 %copy-start.3 = (f32[2,1024]{1,0:T(2,128)S(1)}, f32[2,1024]{1,0:T(2,128)}, u32[]{:S(2)}) copy-start(f32[2,1024]{1,0:T(2,128)} %param.18) | copy-start | bytes 24580
  20.1 15.7 %copy-start.2 = (f32[2,12,512]{2,0,1:T(2,128)S(1)}, f32[2,12,512]{2,0,1:T(2,128)}, u32[]{:S(2)}) copy-start(f32[2,12,512]{2,0,1:T(2,128)} %param.20) | copy-start | bytes 147460
  21.6 21.1 %copy-start.5 = (u32[32]{0:T(128)S(1)}, u32[32]{0:T(128)}, u32[]{:S(2)}) copy-start(u32[32]{0:T(128)} %constant.42) | copy-start | bytes 388
  34.4 9.7 %collective-permute-start = (bf16[12,3584]{1,0:T(8,128)(2,1)S(1)}, bf16[12,3584]{1,0:T(8,128)(2,1)S(1)}, u32[]{:S(2)}, u32[]{:S(2)}) collective-permute-start(bf16[12,3584]{1,0:T(8,128)(2,1)S(1)} %slice.130), channel_id=1, source_target_pairs={{0,1},{1,2},{2,3},{4,5},{5,6},{6,7},{8,9},{9,10},{10,11},{12,13},{... | collective-permute-start | bytes 258056
  44.8 28.2 %copy-start.4 = (u32[32]{0:T(128)S(1)}, u32[32]{0:T(128)}, u32[]{:S(2)}) copy-start(u32[32]{0:T(128)} %constant.46) | copy-start | bytes 388
  44.8 29.9 %copy-start.1 = (bf16[12,1024]{1,0:T(8,128)(2,1)S(1)}, bf16[12,1024]{1,0:T(8,128)(2,1)}, u32[]{:S(2)}) copy-start(bf16[12,1024]{1,0:T(8,128)(2,1)} %param.11) | copy-start | bytes 73732
  71.2 3.3 %collective-permute-start.1 = (bf16[12,1024]{1,0:T(8,128)(2,1)S(1)}, bf16[12,1024]{1,0:T(8,128)(2,1)S(1)}, u32[]{:S(2)}, u32[]{:S(2)}) collective-permute-start(bf16[12,1024]{1,0:T(8,128)(2,1)S(1)} %slice.131), channel_id=1, source_target_pairs={{0,4},{4,8},{8,12},{1,5},{5,9},{9,13},{2,6},{6,10},{10,14},{3,7},{... | collective-permute-start | bytes 73736
  94.0 6.8 %copy-start.7 = (bf16[2,1024,1024]{2,1,0:T(8,128)(2,1)S(1)}, bf16[2,1024,1024]{2,1,0:T(8,128)(2,1)}, u32[]{:S(2)}) copy-start(bf16[2,1024,1024]{2,1,0:T(8,128)(2,1)} %param.17) | copy-start | bytes 12582916
  111.7 2.2 %collective-permute-start.2 = (bf16[12,3584]{1,0:T(8,128)(2,1)S(1)}, bf16[12,3584]{1,0:T(8,128)(2,1)S(1)}, u32[]{:S(2)}, u32[]{:S(2)}) collective-permute-start(bf16[12,3584]{1,0:T(8,128)(2,1)S(1)} %slice.132), channel_id=1, source_target_pairs={{0,1},{1,2},{2,3},{4,5},{5,6},{6,7},{8,9},{9,10},{10,11},{12,13},{... | collective-permute-start | bytes 258056
  114.4 9.8 %slice-start = ((s8[6291456]{0:T(1024)(128)(4,1)}), s8[2097152]{0:T(1024)(128)(4,1)S(1)}, s32[]{:S(2)}) async-start(s8[6291456]{0:T(1024)(128)(4,1)} %bitcast.125), calls=%async_computation | async-start | bytes 4194304
  114.7 9.5 %slice-start.1 = ((s8[6291456]{0:T(1024)(128)(4,1)}), s8[4194304]{0:T(1024)(128)(4,1)S(1)}, s32[]{:S(2)}) async-start(s8[6291456]{0:T(1024)(128)(4,1)} %bitcast.125), calls=%async_computation.1 | async-start | bytes 8388608
  127.4 26.5 %copy-start = (f32[1,12,8,64,128]{4,3,2,1,0:T(8,128)S(1)}, f32[1,12,8,64,128]{4,3,2,1,0:T(8,128)}, u32[]{:S(2)}) copy-start(f32[1,12,8,64,128]{4,3,2,1,0:T(8,128)} %get-tuple-element.2) | copy-start | bytes 9437188
  152.1 7.2 %collective-permute-start.3 = (bf16[12,1024]{1,0:T(8,128)(2,1)S(1)}, bf16[12,1024]{1,0:T(8,128)(2,1)S(1)}, u32[]{:S(2)}, u32[]{:S(2)}) collective-permute-start(bf16[12,1024]{1,0:T(8,128)(2,1)S(1)} %slice.133), channel_id=1, source_target_pairs={{0,4},{4,8},{8,12},{1,5},{5,9},{9,13},{2,6},{6,10},{10,14},{3,7},{... | collective-permute-start | bytes 73736
where the time goes:
time: 161 us; the launch traced here: 160 us
  blocking collectives  103 us (64%)
  other arithmetic  25.1 us (16%)
  matrix products  18.6 us (12%)
  starting transfers between devices  6.12 us (4%)
  local copies, waits for them, and re-layouts  3.67 us (2%)
  between operations  2.47 us (2%)
    unnamed x4, blocking collectives  47.3 us
    all_gather x2, blocking collectives, per_device(): gathered = lax.all_gather(current, 'tp', axis=0, tiled=True)  28.7 us
    dot_general x10, matrix products, per_device(): jnp.dot(scaled_query, matrix[index_of_block], preferred_element_type=jnp....  14.5 us
    all_gather x2, blocking collectives, per_device(): lax.all_gather(gated_out, 'dp', axis=0, tiled=True)  14.3 us
    psum x2, blocking collectives, per_device(): whole_squares = lax.psum(squares, 'dp')  12.6 us
    add x1, other arithmetic, per_device(): decay_rate[:, :, :, None] * state[index_of_block]  9.51 us
    reduce_sum x2, other arithmetic, per_device(): readout = jnp.sum(query_rows[:, :, :, None] * fresh, axis=2)  8.37 us
    unnamed x4, starting transfers between devices  6.12 us
  transfers between devices with their start and end apart: 4, of which 2 were waited for; matrix products, arithmetic and copies ran while one was open for 4% of the time, Pallas kernels for 0%

commit v1 on v0

v1 whole, which is shorter than its diff:
```python
import functools

import jax
import jax.numpy as jnp
from jax import lax
from jax.experimental import pallas as pl
from jax.experimental.pallas import tpu as pltpu
from jax.sharding import PartitionSpec as P

EPSILON = 1e-06
SOFTNESS = 16.0
F32 = jnp.float32
BF16 = jnp.bfloat16


def block_kernel(
    n_tp, n_dp, d_model, head_key, value_channels,
    hidden_ref, gain_ref, out_gain_ref, offset_ref,
    wq_hbm, wk_hbm, wd_hbm, wv_hbm, wg_hbm, wo_hbm, state_hbm,
    hidden_out_ref, new_state_ref,
    wq, wk, wd, wv, wg, wo, state,
    current, gathered, part_send, part_recv, sq_send, sq_recv,
    turned, products, value_buf, gate_buf, decay_buf, readout,
    gated_all, mix_send, mix_recv,
    load_sem, gather_sems, part_sems, sq_sems, gated_sems, mix_sems,
):
    layers, rows, heads = state.shape[0], state.shape[1], state.shape[2]
    pad = current.shape[1]
    width = current.shape[2]
    pieces, piece = part_send.shape[1], part_send.shape[4]
    mix_pieces, mix_piece = mix_send.shape[1], mix_send.shape[4]
    key_cols = heads * head_key
    value_cols = heads * value_channels
    tp = lax.axis_index("tp")
    dp = lax.axis_index("dp")

    sources = (wq_hbm, wk_hbm, wd_hbm, wv_hbm, wg_hbm, wo_hbm, state_hbm)
    targets = (wq, wk, wd, wv, wg, wo, state)

    def load(index, layer):
        return pltpu.make_async_copy(
            sources[index].at[layer], targets[index].at[layer], load_sem.at[index, layer]
        )

    for layer in range(layers):
        for index in (0, 1, 2, 3, 4, 6, 5):
            load(index, layer).start()

    barrier = pltpu.get_barrier_semaphore()
    for j in range(1, n_tp):
        pl.semaphore_signal(
            barrier, inc=1, device_id={"tp": lax.rem(tp + j, n_tp)},
            device_id_type=pl.DeviceIdType.MESH,
        )
    for j in range(1, n_dp):
        pl.semaphore_signal(
            barrier, inc=1, device_id={"dp": lax.rem(dp + j, n_dp)},
            device_id_type=pl.DeviceIdType.MESH,
        )
    current[0, pl.ds(0, rows), :] = hidden_ref[...]
    for layer in range(layers):
        readout[layer] = jnp.zeros_like(readout[layer])
    pl.semaphore_wait(barrier, n_tp + n_dp - 2)

    def remote(src, dst, sems, index, axis, target):
        return pltpu.make_async_remote_copy(
            src_ref=src, dst_ref=dst,
            send_sem=sems.at[(0,) + index], recv_sem=sems.at[(1,) + index],
            device_id={axis: target}, device_id_type=pl.DeviceIdType.MESH,
        )

    pending = []

    for layer in range(layers):
        copies = []
        for j in range(1, n_tp):
            copy = remote(
                current.at[layer], gathered.at[layer, tp], gather_sems, (layer, j - 1),
                "tp", lax.rem(tp + j, n_tp),
            )
            copy.start()
            copies.append(copy)
        gathered[layer, tp] = current[layer]
        for copy in copies:
            copy.wait_recv()
        pending += copies
        widened = gathered[layer].reshape(n_tp * pad, width).astype(F32)
        scaled = (widened * gain_ref[layer, :][None, :]).astype(BF16)
        squares = jnp.sum(widened * widened, axis=1, keepdims=True)
        sq_send[layer] = jnp.broadcast_to(squares, (n_tp * pad, 128)).reshape(n_tp, pad, 128)
        sq_copies = []
        for j in range(1, n_dp):
            to = lax.rem(dp + j, n_dp)
            copy = remote(
                sq_send.at[layer, to], sq_recv.at[layer, j - 1], sq_sems, (layer, j - 1), "dp", to
            )
            copy.start()
            sq_copies.append(copy)

        part_copies = []
        p = 0
        for index, matrix in enumerate((wq, wk, wd, wv, wg)):
            load(index, layer).wait()
            for start in range(0, matrix.shape[2], piece):
                result = jnp.dot(
                    scaled, matrix[layer, :, pl.ds(start, piece)], preferred_element_type=F32
                )
                part_send[layer, p] = result.astype(BF16).reshape(n_dp, pad, piece)
                for j in range(1, n_dp):
                    to = lax.rem(dp + j, n_dp)
                    copy = remote(
                        part_send.at[layer, p, to], part_recv.at[layer, p, j - 1],
                        part_sems, (layer, p, j - 1), "dp", to,
                    )
                    copy.start()
                    part_copies.append(copy)
                p += 1
        pending += sq_copies + part_copies

        for copy in sq_copies:
            copy.wait_recv()
        total_squares = sq_send[layer, dp]
        for j in range(1, n_dp):
            total_squares = total_squares + sq_recv[layer, j - 1]
        inverse = lax.rsqrt(total_squares / d_model + EPSILON)[:, :1]

        def projected(p):
            for j in range(1, n_dp):
                part_copies[p * (n_dp - 1) + j - 1].wait_recv()
            total = part_send[layer, p, dp].astype(F32)
            for j in range(1, n_dp):
                total = total + part_recv[layer, p, j - 1].astype(F32)
            return total * inverse

        def projected_range(first, columns):
            got = [projected(first + i) for i in range(columns // piece)]
            return got[0] if len(got) == 1 else jnp.concatenate(got, axis=1)

        per_key = key_cols // piece
        per_value = value_cols // piece
        query = projected_range(0, key_cols)
        key = projected_range(per_key, key_cols) * head_key ** (-0.5)
        logits = projected_range(2 * per_key, key_cols)
        log_sigmoid = jnp.minimum(logits, 0.0) - jnp.log(1.0 + jnp.exp(-jnp.abs(logits)))
        decay_buf[layer, pl.ds(0, rows), :] = (
            log_sigmoid[:rows] / SOFTNESS + offset_ref[layer]
        )
        decay = jnp.exp(decay_buf[layer])
        stacked = jnp.concatenate(
            [query * decay, key, decay, jnp.zeros((128 - 3 * pad, key_cols), F32)], axis=0
        )
        turned[layer] = stacked.T.reshape(heads, head_key, 128)
        both = query * key
        for h in range(heads):
            own = both[:, h * head_key : (h + 1) * head_key]
            products[layer, h] = jnp.broadcast_to(
                jnp.sum(own, axis=1, keepdims=True), (pad, 128)
            )
        load(6, layer).wait()

        def read_head(h, _):
            columns = turned[layer, h]
            for b in range(rows):
                factor = jnp.broadcast_to(columns[:, b : b + 1], (head_key, value_channels))
                readout[layer, h, pl.ds(b, 1), :] = jnp.sum(
                    factor * state[layer, b, h], axis=0, keepdims=True
                )
            return 0

        lax.fori_loop(0, heads, read_head, 0)

        value_buf[layer] = projected_range(3 * per_key, value_cols)
        gate_buf[layer] = projected_range(3 * per_key + per_value, value_cols)
        for h in range(heads):
            span = slice(h * value_channels, (h + 1) * value_channels)
            got = readout[layer, h] + products[layer, h] * value_buf[layer, :, span]
            gate = gate_buf[layer, :, span]
            normed = got * lax.rsqrt(jnp.mean(got * got, axis=1, keepdims=True) + EPSILON)
            normed = normed * out_gain_ref[layer, span][None, :]
            gated_all[layer, dp, :, span] = (normed * (gate / (1.0 + jnp.exp(-gate)))).astype(BF16)

        copies = []
        for j in range(1, n_dp):
            copy = remote(
                gated_all.at[layer, dp], gated_all.at[layer, dp], gated_sems, (layer, j - 1),
                "dp", lax.rem(dp + j, n_dp),
            )
            copy.start()
            copies.append(copy)

        def renew_head(h, _):
            columns = turned[layer, h]
            values = value_buf[layer, :, pl.ds(pl.multiple_of(h * value_channels, value_channels), value_channels)]
            for b in range(rows):
                shape = (head_key, value_channels)
                keep = jnp.broadcast_to(columns[:, 2 * pad + b : 2 * pad + b + 1], shape)
                add = jnp.broadcast_to(columns[:, pad + b : pad + b + 1], shape)
                new_state_ref[layer, b, h] = keep * state[layer, b, h] + add * values[b : b + 1]
            return 0

        lax.fori_loop(0, heads, renew_head, 0)

        load(5, layer).wait()
        for copy in copies:
            copy.wait_recv()
        pending += copies

        gated = gated_all[layer].reshape(n_dp * pad, value_cols)
        mix_copies = []
        for p in range(mix_pieces):
            result = jnp.dot(
                gated, wo[layer, :, pl.ds(p * mix_piece, mix_piece)], preferred_element_type=F32
            )
            mix_send[layer, p] = result.astype(BF16).reshape(n_tp, pad, mix_piece)
            for j in range(1, n_tp):
                to = lax.rem(tp + j, n_tp)
                copy = remote(
                    mix_send.at[layer, p, to], mix_recv.at[layer, p, j - 1],
                    mix_sems, (layer, p, j - 1), "tp", to,
                )
                copy.start()
                mix_copies.append(copy)
        pending += mix_copies
        for p in range(mix_pieces):
            span = slice(p * mix_piece, (p + 1) * mix_piece)
            for j in range(1, n_tp):
                mix_copies[p * (n_tp - 1) + j - 1].wait_recv()
            total = mix_send[layer, p, tp].astype(F32)
            for j in range(1, n_tp):
                total = total + mix_recv[layer, p, j - 1].astype(F32)
            result = (current[layer, :, span].astype(F32) + total).astype(BF16)
            if layer + 1 < layers:
                current[layer + 1, :, span] = result
            else:
                hidden_out_ref[:, span] = result[:rows]

    for copy in pending:
        copy.wait_send()


def fused(
    n_tp, n_dp, hidden_in, input_norm_gain, w_query, w_key, w_decay, w_value, w_gate,
    out_gain, w_out, decay_offset, state,
):
    layers, rows, heads, head_key, value_channels = state.shape
    width = hidden_in.shape[1]
    pad = -(-rows // 16) * 16
    key_cols, value_cols = w_query.shape[2], w_value.shape[2]
    piece = min(512, key_cols)
    pieces = (3 * key_cols + 2 * value_cols) // piece
    mix_piece = min(512, width)
    mix_pieces = width // mix_piece
    vmem = pl.BlockSpec(memory_space=pltpu.VMEM)
    hbm = pl.BlockSpec(memory_space=pl.ANY)
    return pl.pallas_call(
        functools.partial(
            block_kernel, n_tp, n_dp, width * n_dp, head_key, value_channels
        ),
        out_shape=(
            jax.ShapeDtypeStruct(hidden_in.shape, BF16),
            pltpu.VMEM(state.shape, F32),
        ),
        in_specs=[vmem] * 4 + [hbm] * 7,
        out_specs=(vmem, vmem),
        scratch_shapes=[
            pltpu.VMEM(w_query.shape, BF16),
            pltpu.VMEM(w_key.shape, BF16),
            pltpu.VMEM(w_decay.shape, BF16),
            pltpu.VMEM(w_value.shape, BF16),
            pltpu.VMEM(w_gate.shape, BF16),
            pltpu.VMEM(w_out.shape, BF16),
            pltpu.VMEM(state.shape, F32),
            pltpu.VMEM((layers, pad, width), BF16),
            pltpu.VMEM((layers, n_tp, pad, width), BF16),
            pltpu.VMEM((layers, pieces, n_dp, pad, piece), BF16),
            pltpu.VMEM((layers, pieces, n_dp - 1, pad, piece), BF16),
            pltpu.VMEM((layers, n_dp, pad, 128), F32),
            pltpu.VMEM((layers, n_dp - 1, pad, 128), F32),
            pltpu.VMEM((layers, heads, head_key, 128), F32),
            pltpu.VMEM((layers, heads, pad, 128), F32),
            pltpu.VMEM((layers, pad, value_cols), F32),
            pltpu.VMEM((layers, pad, value_cols), F32),
            pltpu.VMEM((layers, pad, key_cols), F32),
            pltpu.VMEM((layers, heads, pad, value_channels), F32),
            pltpu.VMEM((layers, n_dp, pad, value_cols), BF16),
            pltpu.VMEM((layers, mix_pieces, n_tp, pad, mix_piece), BF16),
            pltpu.VMEM((layers, mix_pieces, n_tp - 1, pad, mix_piece), BF16),
            pltpu.SemaphoreType.DMA((7, layers)),
            pltpu.SemaphoreType.DMA((2, layers, n_tp - 1)),
            pltpu.SemaphoreType.DMA((2, layers, pieces, n_dp - 1)),
            pltpu.SemaphoreType.DMA((2, layers, n_dp - 1)),
            pltpu.SemaphoreType.DMA((2, layers, n_dp - 1)),
            pltpu.SemaphoreType.DMA((2, layers, mix_pieces, n_tp - 1)),
        ],
        compiler_params=pltpu.CompilerParams(
            collective_id=0, has_side_effects=True, vmem_limit_bytes=48 * 1024 * 1024
        ),
    )(
        hidden_in, input_norm_gain, out_gain, decay_offset,
        w_query, w_key, w_decay, w_value, w_gate, w_out, state,
    )


def plain(
    hidden_in, input_norm_gain, w_query, w_key, w_decay, w_value, w_gate,
    out_gain, w_out, decay_offset, state,
):
    layers, rows, heads, head_key, value_channels = state.shape
    key_cols, value_cols = w_query.shape[2], w_value.shape[2]
    d_model = hidden_in.shape[1] * lax.axis_size("dp")
    first = lax.axis_index("dp") * rows
    current, states = hidden_in, []
    for layer in range(layers):
        widened = lax.all_gather(current, "tp", axis=0, tiled=True).astype(F32)
        squares = lax.psum(jnp.sum(widened * widened, axis=1), "dp")
        scaled = (widened * input_norm_gain[layer][None, :]).astype(BF16)
        partial = jnp.concatenate(
            [
                jnp.dot(scaled, matrix[layer], preferred_element_type=F32)
                for matrix in (w_query, w_key, w_decay, w_value, w_gate)
            ],
            axis=1,
        ).astype(BF16)
        summed = lax.psum_scatter(partial, "dp", scatter_dimension=0, tiled=True).astype(F32)
        own = lax.dynamic_slice_in_dim(squares, first, rows)
        projected = summed * lax.rsqrt(own / d_model + EPSILON)[:, None]
        query, key, logits, value, gate = jnp.split(
            projected,
            [key_cols, 2 * key_cols, 3 * key_cols, 3 * key_cols + value_cols],
            axis=1,
        )
        decay = jnp.exp(jax.nn.log_sigmoid(logits) / SOFTNESS + decay_offset[layer])
        per_key, per_value = (rows, heads, head_key), (rows, heads, value_channels)
        fresh = (
            decay.reshape(per_key)[..., None] * state[layer]
            + (key * head_key ** (-0.5)).reshape(per_key)[..., None]
            * value.reshape(per_value)[:, :, None, :]
        )
        got = jnp.sum(query.reshape(per_key)[..., None] * fresh, axis=2)
        got = got * lax.rsqrt(jnp.mean(got * got, axis=2, keepdims=True) + EPSILON)
        got = got * out_gain[layer].reshape(heads, value_channels)[None]
        gated = (got * jax.nn.silu(gate.reshape(per_value))).reshape(rows, value_cols).astype(BF16)
        mixed = jnp.dot(
            lax.all_gather(gated, "dp", axis=0, tiled=True), w_out[layer],
            preferred_element_type=F32,
        ).astype(BF16)
        mine = lax.psum_scatter(mixed, "tp", scatter_dimension=0, tiled=True).astype(F32)
        current = (current.astype(F32) + mine).astype(BF16)
        states.append(fresh)
    return current, jnp.stack(states)


def solution(mesh):
    n_tp, n_dp = mesh.shape["tp"], mesh.shape["dp"]

    def per_device(hidden_in, *rest):
        state = rest[-1]
        aligned = rest[1].shape[2] % 128 == 0 and hidden_in.shape[1] % 128 == 0
        if n_tp > 1 and n_tp == n_dp and aligned and 3 * state.shape[1] <= 96:
            return fused(n_tp, n_dp, hidden_in, *rest)
        return plain(hidden_in, *rest)

    return jax.shard_map(
        per_device,
        mesh=mesh,
        in_specs=(
            P(("grp", "tp"), "dp"),
            P(None, "dp"),
            P(None, "dp", "tp"),
            P(None, "dp", "tp"),
            P(None, "dp", "tp"),
            P(None, "dp", "tp"),
            P(None, "dp", "tp"),
            P(None, "tp"),
            P(None, "tp", "dp"),
            P(None, ("grp", "dp"), "tp"),
            P(None, ("grp", "dp"), "tp", None, None),
        ),
        out_specs=(P(("grp", "tp"), "dp"), P(None, ("grp", "dp"), "tp", None, None)),
        check_vma=False,
    )
```

time: 161 us -> 51.7 us (0.32)
  blocking collectives: 103 us -> 0 us
  Pallas kernels: 0 us -> 46.1 us
  other arithmetic: 25.1 us -> 0 us
  matrix products: 18.6 us -> 0 us
  starting transfers between devices: 6.12 us -> 0 us
  between operations: 2.47 us -> 0.65 us
    unnamed x4 -> x0, blocking collectives: 47.3 us -> none
    pallas_call x0 -> x1, Pallas kernels: none -> 46.1 us  [fused(): pl.pallas_call(functools.partial(block_kernel, n_tp, n_dp, width * n_dp,...]
    all_gather x4 -> x0, blocking collectives: 43.1 us -> none  [the longest x2 28.7 us: per_device(): gathered = lax.all_gather(current, 'tp', axis=0, tiled=True)]
    dot_general x12 -> x0, matrix products: 18.6 us -> none  [the longest x10 14.5 us: per_device(): jnp.dot(scaled_query, matrix[index_of_block], preferred_element_type=jnp....]
    psum x2 -> x0, blocking collectives: 12.6 us -> none  [per_device(): whole_squares = lax.psum(squares, 'dp')]
    add x1 -> x0, other arithmetic: 9.51 us -> none  [per_device(): decay_rate[:, :, :, None] * state[index_of_block]]
    reduce_sum x6 -> x0, other arithmetic: 8.79 us -> none  [the longest x2 8.37 us: per_device(): readout = jnp.sum(query_rows[:, :, :, None] * fresh, axis=2)]
    unnamed x4 -> x0, starting transfers between devices: 6.12 us -> none
  transfers between devices with their start and end apart: 4 -> 0, of which waited for: 2 -> 0; matrix products, arithmetic and copies ran while one was open for 4% -> 0% of each run, Pallas kernels for 0% -> 0%
where the time goes in v1:
time: 51.7 us; the launch traced here: 51.5 us
  Pallas kernels  46.1 us (89%)
  local copies, waits for them, and re-layouts  4.76 us (9%)
  between operations  0.65 us (1%)
    pallas_call x1, Pallas kernels, fused(): pl.pallas_call(functools.partial(block_kernel, n_tp, n_dp, width * n_dp,...  46.1 us
    unnamed x5, local copies, waits for them, and re-layouts  4.76 us

profile of v1, /device:TPU:0, one launch (start us, length us, event | category | flops | bytes accessed | tf_op | source)
XLA Modules:
  0.0 51.5 jit_solution(18008295211245223063)
XLA Ops:
  0.6 1.4 %copy.13.offset_ref = f32[2,12,512]{2,1,0:T(8,128)} copy(f32[2,12,512]{2,0,1:T(2,128)} %param.20) | data formatting | bytes 98304 | tf_op args[9]
  2.1 46.1 %shard_map.122 = (bf16[12,1024]{1,0:T(8,128)(2,1)}, f32[2,12,8,64,128]{4,3,2,1,0:T(8,128)S(1)}) custom-call(bf16[12,1024]{1,0:T(8,128)(2,1)} %hidden_ref.1, f32[2,1024]{1,0:T(2,128)} %gain_ref.1, f32[2,1024]{1,0:T(2,128)} %out_gain_ref.1, f32[2,12,512]{2,1,0:T(8,128)} %copy.13.offset_ref, bf16[2,1024,512]{2,1,0:T(8,128)(2,1)} %wq_hbm.1, ...), custom_call_target="tpu_custom_call" | custom-call | tf_op jit(solution)/shard_map/pallas_call | solution.py:255
  48.1 0.0 copy-start
  48.2 2.7 %copy.16 = f32[2,12,8,64,128]{4,3,2,1,0:T(8,128)} copy(f32[2,12,8,64,128]{4,3,2,1,0:T(8,128)S(1)} %get-tuple-element.3) | data formatting | bytes 12582912
  50.9 0.0 copy-done
  50.9 0.6 %copy.17 = bf16[12,1024]{1,0:T(8,128)(2,1)} copy(bf16[12,1024]{1,0:T(8,128)(2,1)S(1)} %copy-done) | data formatting | bytes 49152
Async XLA Ops:
  48.1 2.7 %copy-start = (bf16[12,1024]{1,0:T(8,128)(2,1)S(1)}, bf16[12,1024]{1,0:T(8,128)(2,1)}, u32[]{:S(2)}) copy-start(bf16[12,1024]{1,0:T(8,128)(2,1)} %get-tuple-element.6) | copy-start | bytes 73732

commit v2 on v1

--- a/solution.py
+++ b/solution.py
@@ -13,8 +13,29 @@
 BF16 = jnp.bfloat16
 
 
+def pack(block, rows):
+    if block.shape[0] != 16 or rows > 12 or block.shape[1] % 256:
+        return block
+    half = block.shape[1] // 2
+    tail = jnp.concatenate([block[8:12, :half], block[8:12, half:]], axis=0)
+    return jnp.concatenate([block[:8], tail], axis=1)
+
+
+def unpack(block, rows, columns):
+    if block.shape[1] == columns:
+        return block
+    tail = jnp.concatenate([block[:4, columns:], block[4:, columns:]], axis=1)
+    return jnp.concatenate([block[:, :columns], tail, jnp.zeros_like(tail)], axis=0)
+
+
+def packed_shape(pad, rows, columns):
+    if pad != 16 or rows > 12 or columns % 256:
+        return pad, columns
+    return 8, columns // 2 * 3
+
+
 def block_kernel(
-    n_tp, n_dp, d_model, head_key, value_channels,
+    n_tp, n_dp, d_model, head_key, value_channels, piece, mix_piece,
     hidden_ref, gain_ref, out_gain_ref, offset_ref,
     wq_hbm, wk_hbm, wd_hbm, wv_hbm, wg_hbm, wo_hbm, state_hbm,
     hidden_out_ref, new_state_ref,
@@ -27,8 +48,7 @@
     layers, rows, heads = state.shape[0], state.shape[1], state.shape[2]
     pad = current.shape[1]
     width = current.shape[2]
-    pieces, piece = part_send.shape[1], part_send.shape[4]
-    mix_pieces, mix_piece = mix_send.shape[1], mix_send.shape[4]
+    mix_pieces = mix_send.shape[1]
     key_cols = heads * head_key
     value_cols = heads * value_channels
     tp = lax.axis_index("tp")
@@ -72,19 +92,21 @@
     pending = []
 
     for layer in range(layers):
+        gathered[layer, tp] = pack(current[layer].astype(F32), rows).astype(BF16)
         copies = []
         for j in range(1, n_tp):
             copy = remote(
-                current.at[layer], gathered.at[layer, tp], gather_sems, (layer, j - 1),
+                gathered.at[layer, tp], gathered.at[layer, tp], gather_sems, (layer, j - 1),
                 "tp", lax.rem(tp + j, n_tp),
             )
             copy.start()
             copies.append(copy)
-        gathered[layer, tp] = current[layer]
         for copy in copies:
             copy.wait_recv()
         pending += copies
-        widened = gathered[layer].reshape(n_tp * pad, width).astype(F32)
+        widened = jnp.concatenate(
+            [unpack(gathered[layer, s].astype(F32), rows, width) for s in range(n_tp)], axis=0
+        )
         scaled = (widened * gain_ref[layer, :][None, :]).astype(BF16)
         squares = jnp.sum(widened * widened, axis=1, keepdims=True)
         sq_send[layer] = jnp.broadcast_to(squares, (n_tp * pad, 128)).reshape(n_tp, pad, 128)
@@ -105,7 +127,9 @@
                 result = jnp.dot(
                     scaled, matrix[layer, :, pl.ds(start, piece)], preferred_element_type=F32
                 )
-                part_send[layer, p] = result.astype(BF16).reshape(n_dp, pad, piece)
+                for s in range(n_dp):
+                    block = result[s * pad : (s + 1) * pad]
+                    part_send[layer, p, s] = pack(block, rows).astype(BF16)
                 for j in range(1, n_dp):
                     to = lax.rem(dp + j, n_dp)
                     copy = remote(
@@ -130,7 +154,7 @@
             total = part_send[layer, p, dp].astype(F32)
             for j in range(1, n_dp):
                 total = total + part_recv[layer, p, j - 1].astype(F32)
-            return total * inverse
+            return unpack(total, rows, piece) * inverse
 
         def projected_range(first, columns):
             got = [projected(first + i) for i in range(columns // piece)]
@@ -143,7 +167,7 @@
         logits = projected_range(2 * per_key, key_cols)
         log_sigmoid = jnp.minimum(logits, 0.0) - jnp.log(1.0 + jnp.exp(-jnp.abs(logits)))
         decay_buf[layer, pl.ds(0, rows), :] = (
-            log_sigmoid[:rows] / SOFTNESS + offset_ref[layer]
+            log_sigmoid[:rows] / SOFTNESS + offset_ref[:, layer, :]
         )
         decay = jnp.exp(decay_buf[layer])
         stacked = jnp.concatenate(
@@ -171,13 +195,15 @@
 
         value_buf[layer] = projected_range(3 * per_key, value_cols)
         gate_buf[layer] = projected_range(3 * per_key + per_value, value_cols)
+        gated_heads = []
         for h in range(heads):
             span = slice(h * value_channels, (h + 1) * value_channels)
             got = readout[layer, h] + products[layer, h] * value_buf[layer, :, span]
             gate = gate_buf[layer, :, span]
             normed = got * lax.rsqrt(jnp.mean(got * got, axis=1, keepdims=True) + EPSILON)
             normed = normed * out_gain_ref[layer, span][None, :]
-            gated_all[layer, dp, :, span] = (normed * (gate / (1.0 + jnp.exp(-gate)))).astype(BF16)
+            gated_heads.append(normed * (gate / (1.0 + jnp.exp(-gate))))
+        gated_all[layer, dp] = pack(jnp.concatenate(gated_heads, axis=1), rows).astype(BF16)
 
         copies = []
         for j in range(1, n_dp):
@@ -205,13 +231,21 @@
             copy.wait_recv()
         pending += copies
 
-        gated = gated_all[layer].reshape(n_dp * pad, value_cols)
+        gated = jnp.concatenate(
+            [
+                unpack(gated_all[layer, s].astype(F32), rows, value_cols).astype(BF16)
+                for s in range(n_dp)
+            ],
+            axis=0,
+        )
         mix_copies = []
         for p in range(mix_pieces):
             result = jnp.dot(
                 gated, wo[layer, :, pl.ds(p * mix_piece, mix_piece)], preferred_element_type=F32
             )
-            mix_send[layer, p] = result.astype(BF16).reshape(n_tp, pad, mix_piece)
+            for s in range(n_tp):
+                block = result[s * pad : (s + 1) * pad]
+                mix_send[layer, p, s] = pack(block, rows).astype(BF16)
             for j in range(1, n_tp):
                 to = lax.rem(tp + j, n_tp)
                 copy = remote(
@@ -228,6 +262,7 @@
             total = mix_send[layer, p, tp].astype(F32)
             for j in range(1, n_tp):
                 total = total + mix_recv[layer, p, j - 1].astype(F32)
+            total = unpack(total, rows, mix_piece)
             result = (current[layer, :, span].astype(F32) + total).astype(BF16)
             if layer + 1 < layers:
                 current[layer + 1, :, span] = result
@@ -250,11 +285,14 @@
     pieces = (3 * key_cols + 2 * value_cols) // piece
     mix_piece = min(512, width)
     mix_pieces = width // mix_piece
+    part_shape = packed_shape(pad, rows, piece)
+    mix_shape = packed_shape(pad, rows, mix_piece)
     vmem = pl.BlockSpec(memory_space=pltpu.VMEM)
     hbm = pl.BlockSpec(memory_space=pl.ANY)
     return pl.pallas_call(
         functools.partial(
-            block_kernel, n_tp, n_dp, width * n_dp, head_key, value_channels
+            block_kernel, n_tp, n_dp, width * n_dp, head_key, value_channels,
+            piece, mix_piece,
         ),
         out_shape=(
             jax.ShapeDtypeStruct(hidden_in.shape, BF16),
@@ -271,9 +309,9 @@
             pltpu.VMEM(w_out.shape, BF16),
             pltpu.VMEM(state.shape, F32),
             pltpu.VMEM((layers, pad, width), BF16),
-            pltpu.VMEM((layers, n_tp, pad, width), BF16),
-            pltpu.VMEM((layers, pieces, n_dp, pad, piece), BF16),
-            pltpu.VMEM((layers, pieces, n_dp - 1, pad, piece), BF16),
+            pltpu.VMEM((layers, n_tp) + packed_shape(pad, rows, width), BF16),
+            pltpu.VMEM((layers, pieces, n_dp) + part_shape, BF16),
+            pltpu.VMEM((layers, pieces, n_dp - 1) + part_shape, BF16),
             pltpu.VMEM((layers, n_dp, pad, 128), F32),
             pltpu.VMEM((layers, n_dp - 1, pad, 128), F32),
             pltpu.VMEM((layers, heads, head_key, 128), F32),
@@ -282,9 +320,9 @@
             pltpu.VMEM((layers, pad, value_cols), F32),
             pltpu.VMEM((layers, pad, key_cols), F32),
             pltpu.VMEM((layers, heads, pad, value_channels), F32),
-            pltpu.VMEM((layers, n_dp, pad, value_cols), BF16),
-            pltpu.VMEM((layers, mix_pieces, n_tp, pad, mix_piece), BF16),
-            pltpu.VMEM((layers, mix_pieces, n_tp - 1, pad, mix_piece), BF16),
+            pltpu.VMEM((layers, n_dp) + packed_shape(pad, rows, value_cols), BF16),
+            pltpu.VMEM((layers, mix_pieces, n_tp) + mix_shape, BF16),
+            pltpu.VMEM((layers, mix_pieces, n_tp - 1) + mix_shape, BF16),
             pltpu.SemaphoreType.DMA((7, layers)),
             pltpu.SemaphoreType.DMA((2, layers, n_tp - 1)),
             pltpu.SemaphoreType.DMA((2, layers, pieces, n_dp - 1)),
@@ -296,7 +334,7 @@
             collective_id=0, has_side_effects=True, vmem_limit_bytes=48 * 1024 * 1024
         ),
     )(
-        hidden_in, input_norm_gain, out_gain, decay_offset,
+        hidden_in, input_norm_gain, out_gain, decay_offset.transpose(1, 0, 2),
         w_query, w_key, w_decay, w_value, w_gate, w_out, state,
     )
 

time: 51.7 us -> 47.4 us (0.917)
  Pallas kernels: 46.1 us -> 43.2 us
  local copies, waits for them, and re-layouts: 4.76 us -> 3.32 us
    pallas_call x1, Pallas kernels: 46.1 us -> 43.2 us  [fused(): pl.pallas_call(functools.partial(block_kernel, n_tp, n_dp, width * n_dp,...]
    unnamed x5 -> x4, local copies, waits for them, and re-layouts: 4.76 us -> 3.32 us
where the time goes in v2:
time: 47.4 us; the launch traced here: 47.2 us
  Pallas kernels  43.2 us (91%)
  local copies, waits for them, and re-layouts  3.32 us (7%)
  between operations  0.65 us (1%)
    pallas_call x1, Pallas kernels, fused(): pl.pallas_call(functools.partial(block_kernel, n_tp, n_dp, width * n_dp,...  43.2 us
    unnamed x4, local copies, waits for them, and re-layouts  3.32 us

profile of v2, /device:TPU:0, one launch (start us, length us, event | category | flops | bytes accessed | tf_op | source)
XLA Modules:
  0.0 47.2 jit_solution(10091433173811424732)
XLA Ops:
  0.6 43.2 %shard_map.122 = (bf16[12,1024]{1,0:T(8,128)(2,1)}, f32[2,12,8,64,128]{4,3,2,1,0:T(8,128)S(1)}) custom-call(bf16[12,1024]{1,0:T(8,128)(2,1)} %hidden_ref.1, f32[2,1024]{1,0:T(2,128)} %gain_ref.1, f32[2,1024]{1,0:T(2,128)} %out_gain_ref.1, f32[12,2,512]{2,1,0:T(2,128)} %bitcast.1, bf16[2,1024,512]{2,1,0:T(8,128)(2,1)} %wq_hbm.1, ...), custom_call_target="tpu_custom_call" | custom-call | tf_op jit(solution)/shard_map/pallas_call | solution.py:292
  43.9 0.0 copy-start
  43.9 2.7 %copy.15 = f32[2,12,8,64,128]{4,3,2,1,0:T(8,128)} copy(f32[2,12,8,64,128]{4,3,2,1,0:T(8,128)S(1)} %get-tuple-element.3) | data formatting | bytes 12582912
  46.6 0.0 copy-done
  46.6 0.6 %copy.16 = bf16[12,1024]{1,0:T(8,128)(2,1)} copy(bf16[12,1024]{1,0:T(8,128)(2,1)S(1)} %copy-done) | data formatting | bytes 49152
Async XLA Ops:
  43.9 2.7 %copy-start = (bf16[12,1024]{1,0:T(8,128)(2,1)S(1)}, bf16[12,1024]{1,0:T(8,128)(2,1)}, u32[]{:S(2)}) copy-start(bf16[12,1024]{1,0:T(8,128)(2,1)} %get-tuple-element.6) | copy-start | bytes 73732

commit v3 on v2

--- a/solution.py
+++ b/solution.py
@@ -47,7 +47,6 @@
 ):
     layers, rows, heads = state.shape[0], state.shape[1], state.shape[2]
     pad = current.shape[1]
-    width = current.shape[2]
     mix_pieces = mix_send.shape[1]
     key_cols = heads * head_key
     value_cols = heads * value_channels
@@ -91,21 +90,41 @@
 
     pending = []
 
-    for layer in range(layers):
-        gathered[layer, tp] = pack(current[layer].astype(F32), rows).astype(BF16)
-        copies = []
+    def send_features(layer, p):
+        block = current[layer, :, pl.ds(p * mix_piece, mix_piece)].astype(F32)
+        gathered[layer, p, tp] = pack(block, rows).astype(BF16)
+        sent = []
         for j in range(1, n_tp):
             copy = remote(
-                gathered.at[layer, tp], gathered.at[layer, tp], gather_sems, (layer, j - 1),
-                "tp", lax.rem(tp + j, n_tp),
+                gathered.at[layer, p, tp], gathered.at[layer, p, tp], gather_sems,
+                (layer, p, j - 1), "tp", lax.rem(tp + j, n_tp),
             )
             copy.start()
-            copies.append(copy)
+            sent.append(copy)
+        return sent
+
+    feature_copies = []
+    for p in range(mix_pieces):
+        feature_copies += send_features(0, p)
+
+    for layer in range(layers):
+        copies = feature_copies
+        feature_copies = []
         for copy in copies:
             copy.wait_recv()
         pending += copies
         widened = jnp.concatenate(
-            [unpack(gathered[layer, s].astype(F32), rows, width) for s in range(n_tp)], axis=0
+            [
+                jnp.concatenate(
+                    [
+                        unpack(gathered[layer, p, s].astype(F32), rows, mix_piece)
+                        for p in range(mix_pieces)
+                    ],
+                    axis=1,
+                )
+                for s in range(n_tp)
+            ],
+            axis=0,
         )
         scaled = (widened * gain_ref[layer, :][None, :]).astype(BF16)
         squares = jnp.sum(widened * widened, axis=1, keepdims=True)
@@ -266,6 +285,7 @@
             result = (current[layer, :, span].astype(F32) + total).astype(BF16)
             if layer + 1 < layers:
                 current[layer + 1, :, span] = result
+                feature_copies += send_features(layer + 1, p)
             else:
                 hidden_out_ref[:, span] = result[:rows]
 
@@ -309,7 +329,7 @@
             pltpu.VMEM(w_out.shape, BF16),
             pltpu.VMEM(state.shape, F32),
             pltpu.VMEM((layers, pad, width), BF16),
-            pltpu.VMEM((layers, n_tp) + packed_shape(pad, rows, width), BF16),
+            pltpu.VMEM((layers, mix_pieces, n_tp) + mix_shape, BF16),
             pltpu.VMEM((layers, pieces, n_dp) + part_shape, BF16),
             pltpu.VMEM((layers, pieces, n_dp - 1) + part_shape, BF16),
             pltpu.VMEM((layers, n_dp, pad, 128), F32),
@@ -324,7 +344,7 @@
             pltpu.VMEM((layers, mix_pieces, n_tp) + mix_shape, BF16),
             pltpu.VMEM((layers, mix_pieces, n_tp - 1) + mix_shape, BF16),
             pltpu.SemaphoreType.DMA((7, layers)),
-            pltpu.SemaphoreType.DMA((2, layers, n_tp - 1)),
+            pltpu.SemaphoreType.DMA((2, layers, mix_pieces, n_tp - 1)),
             pltpu.SemaphoreType.DMA((2, layers, pieces, n_dp - 1)),
             pltpu.SemaphoreType.DMA((2, layers, n_dp - 1)),
             pltpu.SemaphoreType.DMA((2, layers, n_dp - 1)),

time: 47.4 us -> 47 us (level)
  no operation moved by 1% of the time
where the time goes in v3:
time: 47 us; the launch traced here: 46.8 us
  Pallas kernels  42.8 us (91%)
  local copies, waits for them, and re-layouts  3.32 us (7%)
  between operations  0.65 us (1%)
    pallas_call x1, Pallas kernels, fused(): pl.pallas_call(functools.partial(block_kernel, n_tp, n_dp, width * n_dp,...  42.8 us
    unnamed x4, local copies, waits for them, and re-layouts  3.32 us

profile of v3, /device:TPU:0, one launch (start us, length us, event | category | flops | bytes accessed | tf_op | source)
XLA Modules:
  0.0 46.8 jit_solution(16544122373267611901)
XLA Ops:
  0.6 42.8 %shard_map.122 = (bf16[12,1024]{1,0:T(8,128)(2,1)}, f32[2,12,8,64,128]{4,3,2,1,0:T(8,128)S(1)}) custom-call(bf16[12,1024]{1,0:T(8,128)(2,1)} %hidden_ref.1, f32[2,1024]{1,0:T(2,128)} %gain_ref.1, f32[2,1024]{1,0:T(2,128)} %out_gain_ref.1, f32[12,2,512]{2,1,0:T(2,128)} %bitcast.1, bf16[2,1024,512]{2,1,0:T(8,128)(2,1)} %wq_hbm.1, ...), custom_call_target="tpu_custom_call" | custom-call | tf_op jit(solution)/shard_map/pallas_call | solution.py:312
  43.5 0.0 copy-start
  43.5 2.7 %copy.15 = f32[2,12,8,64,128]{4,3,2,1,0:T(8,128)} copy(f32[2,12,8,64,128]{4,3,2,1,0:T(8,128)S(1)} %get-tuple-element.3) | data formatting | bytes 12582912
  46.2 0.0 copy-done
  46.2 0.6 %copy.16 = bf16[12,1024]{1,0:T(8,128)(2,1)} copy(bf16[12,1024]{1,0:T(8,128)(2,1)S(1)} %copy-done) | data formatting | bytes 49152
Async XLA Ops:
  43.5 2.7 %copy-start = (bf16[12,1024]{1,0:T(8,128)(2,1)S(1)}, bf16[12,1024]{1,0:T(8,128)(2,1)}, u32[]{:S(2)}) copy-start(bf16[12,1024]{1,0:T(8,128)(2,1)} %get-tuple-element.6) | copy-start | bytes 73732
